TPU v7x, 32 devices: a whole 2x2x4 slice. The times are simulated.
32 devices in a mesh: fs: 16 (over z, x, core), tp: 2 (over y).
Axes of the slice: x: 2, y: 2, z: 4, core: 2. Of those that a mesh axis runs over, the one named last changes fastest.
Arguments:
- normed_input: bfloat16 [8192, 2048], P('fs'), may hold values from -6 to 6
- value_cotangent: bfloat16 [8192, 2048], P('fs', 'tp'), may hold values from -6 to 6
- gated_output: bfloat16 [8192, 2048], P('fs', 'tp'), may hold values from -6 to 6
- layer_cotangent: bfloat16 [8192, 2048], P('fs'), may hold values from -6 to 6
- factor_value: bfloat16 [2048, 256], P('fs'), may hold values from -4 to 4, as said below
- factor_output: bfloat16 [2048, 256], P('fs'), may hold values from -4 to 4, as said below
- weight_value: float32 [2048, 2048], P('fs', 'tp'), may hold values from -0.125 to 0.125
- weight_output: float32 [2048, 2048], P('tp', 'fs'), may hold values from -0.125 to 0.125
- first_value: float32 [256, 2048], P('fs', 'tp'), may hold values from -2048 to 2048
- second_value: float32 [256, 2048], P('fs', 'tp'), may hold values from 32768 to 524288
- first_output: float32 [256, 2048], P('fs', 'tp'), may hold values from -2048 to 2048
- second_output: float32 [256, 2048], P('fs', 'tp'), may hold values from 32768 to 524288
Outputs:
- step_value: float32 [2048, 2048], P('fs', 'tp')
- step_output: float32 [2048, 2048], P('tp', 'fs')
- next_weight_value: float32 [2048, 2048], P('fs', 'tp')
- next_weight_output: float32 [2048, 2048], P('tp', 'fs')
- next_first_value: float32 [256, 2048], P('fs', 'tp')
- next_second_value: float32 [256, 2048], P('fs', 'tp')
- next_first_output: float32 [256, 2048], P('fs', 'tp')
- next_second_output: float32 [256, 2048], P('fs', 'tp')
- copy_value: bfloat16 [2048, 2048], P(None, 'tp')
- copy_output: bfloat16 [2048, 2048], P('tp')
Inputs may be any that keep to these rules, and one draw needn't show every extreme that they name: factor_value has full rank. factor_output has full rank.
All inputs are finite; a program needn't handle non-finite values.
Results may differ from a plain program's by a relative error of at most 0.0039.
Values may be sent and summed in bfloat16 or wider, within the bound.
A program may use at most 64 MiB of HBM per device.

v0:
```python
import jax
import jax.numpy as jnp
from jax import lax
from jax.sharding import PartitionSpec as P

D = 2048
WIDTH = 2048


def gram_times(gram_matrix, directions):
    gram_high = gram_matrix.astype(jnp.bfloat16)
    gram_low = (gram_matrix - gram_high.astype(jnp.float32)).astype(jnp.bfloat16)
    return jnp.dot(gram_high, directions, preferred_element_type=jnp.float32) + jnp.dot(
        gram_low, directions, preferred_element_type=jnp.float32
    )


def body(
    normed_input,
    value_cotangent,
    gated_output,
    layer_cotangent,
    factor_value,
    factor_output,
    weight_value,
    weight_output,
    first_value,
    second_value,
    first_output,
    second_output,
):
    col_count = value_cotangent.shape[1]
    inner = (((0,), (0,)), ((), ()))
    pieces = (
        lax.all_gather(factor_value, "fs", axis=0, tiled=True),
        lax.all_gather(factor_output, "fs", axis=0, tiled=True),
    )
    piece_value, piece_output = pieces
    span_input = normed_input
    span_cotan = layer_cotangent
    gram_value = lax.dot_general(pieces[0], pieces[0], inner, preferred_element_type=jnp.float32)
    gram_output = lax.dot_general(pieces[1], pieces[1], inner, preferred_element_type=jnp.float32)
    projected_input = jnp.dot(span_input, piece_value, preferred_element_type=jnp.float32).astype(
        jnp.bfloat16
    )
    projected_cotangent = jnp.dot(
        span_cotan, piece_output, preferred_element_type=jnp.float32
    ).astype(jnp.bfloat16)
    span_input = projected_input
    span_cotan = projected_cotangent
    term_value = lax.dot_general(
        span_input, value_cotangent, inner, preferred_element_type=jnp.float32
    )
    term_output = lax.dot_general(
        span_cotan, gated_output, inner, preferred_element_type=jnp.float32
    )
    low_rank = lax.psum_scatter(
        jnp.concatenate([term_value, term_output], axis=1), "fs", scatter_dimension=0, tiled=True
    )
    low_value = low_rank[:, :col_count]
    low_output = low_rank[:, col_count:]
    next_first_value = 0.9 * first_value + 0.1 * low_value
    next_second_value = 0.95 * second_value + 0.05 * low_value * low_value
    next_first_output = 0.9 * first_output + 0.1 * low_output
    next_second_output = 0.95 * second_output + 0.05 * low_output * low_output
    direction_value = (next_first_value * lax.rsqrt(next_second_value)).astype(jnp.bfloat16)
    direction_output = (next_first_output * lax.rsqrt(next_second_output)).astype(jnp.bfloat16)
    gathered_value, gathered_output = (
        lax.all_gather(direction_value, "fs", axis=0, tiled=True),
        lax.all_gather(direction_output, "fs", axis=0, tiled=True),
    )
    update_value = jnp.dot(factor_value, gathered_value, preferred_element_type=jnp.float32)
    update_output = lax.dot_general(
        gathered_output, factor_output, (((0,), (1,)), ((), ())), preferred_element_type=jnp.float32
    )
    square_value = jnp.sum(
        gathered_value.astype(jnp.float32) * gram_times(gram_value, gathered_value)
    )
    square_output = jnp.sum(
        gathered_output.astype(jnp.float32) * gram_times(gram_output, gathered_output)
    )
    total_value, total_output = lax.psum((square_value, square_output), "tp")
    entries = D * WIDTH
    step_value = update_value * lax.rsqrt(total_value / entries + 1e-06)
    step_output = update_output * lax.rsqrt(total_output / entries + 1e-06)
    next_weight_value = weight_value - 0.02 * step_value
    next_weight_output = weight_output - 0.02 * step_output
    half_value = next_weight_value.astype(jnp.bfloat16)
    half_output = next_weight_output.astype(jnp.bfloat16)
    copy_value, copy_output = (
        lax.all_gather(half_value, "fs", axis=0, tiled=True),
        lax.all_gather(half_output, "fs", axis=1, tiled=True),
    )
    return (
        step_value,
        step_output,
        next_weight_value,
        next_weight_output,
        next_first_value,
        next_second_value,
        next_first_output,
        next_second_output,
        copy_value,
        copy_output,
    )


def solution(mesh):
    placed = (
        P("fs", None),
        P("fs", "tp"),
        P("fs", "tp"),
        P("fs", None),
        P("fs", None),
        P("fs", None),
        P("fs", "tp"),
        P("tp", "fs"),
        P("fs", "tp"),
        P("fs", "tp"),
        P("fs", "tp"),
        P("fs", "tp"),
    )
    return jax.shard_map(
        body,
        mesh=mesh,
        in_specs=placed,
        out_specs=(
            P("fs", "tp"),
            P("tp", "fs"),
            P("fs", "tp"),
            P("tp", "fs"),
            P("fs", "tp"),
            P("fs", "tp"),
            P("fs", "tp"),
            P("fs", "tp"),
            P(None, "tp"),
            P("tp", None),
        ),
        check_vma=False,
    )
```

profile of v0, /device:TPU:9, one launch (start us, length us, event | category | flops | bytes accessed | tf_op | source)
XLA Modules:
  0.0 326.1 jit_solution(14177453045833276398)
XLA Ops:
  7.2 0.0 copy-start
  7.2 0.0 all-gather.7.cloned.1.call-start
  7.2 0.7 all-gather.7.cloned.1.call-update
  7.9 0.0 all-gather.5.cloned.1.call-start
  8.0 0.7 all-gather.5.cloned.1.call-update
  8.7 0.0 reduce-scatter.2.cloned.1.call-start
  8.7 39.8 %all-gather.7.cloned.1.call-done = bf16[2048,256]{1,0:T(8,128)(2,1)} async-done(((bf16[128,256]{1,0:T(8,128)(2,1)}), bf16[2048,256]{1,0:T(8,128)(2,1)}) %all-gather.7.cloned.1.call-update) | async-done | bytes 1048592 | tf_op jit(solution)/shard_map/all_gather | solution.py:36
  48.6 0.0 copy-done
  48.6 3.1 fusion.4
  51.7 35.9 %all-gather.5.cloned.1.call-done = bf16[2048,256]{1,0:T(8,128)(2,1)} async-done(((bf16[128,256]{1,0:T(8,128)(2,1)}), bf16[2048,256]{1,0:T(8,128)(2,1)}) %all-gather.5.cloned.1.call-update) | async-done | bytes 1048592 | tf_op jit(solution)/shard_map/all_gather | solution.py:35
  87.6 4.7 %fusion.3 = f32[256,1024]{1,0:T(8,128)} fusion(bf16[512,1024]{1,0:T(8,128)(2,1)} %param.13, bf16[512,2048]{1,0:T(8,128)(2,1)} %param.12, bf16[2048,256]{1,0:T(8,128)(2,1)} %all-gather.5.cloned.1.call-done), kind=kOutput, calls=%fused_computation.10 | convolution fusion | flops 805437440 | bytes 5242880 | tf_op jit(solution)/shard_map/dot_general | solution.py:51
  92.3 2.7 pad_maximum_fusion
  95.0 0.0 copy-start.1
  95.0 0.0 reduce-scatter.2.cloned.1.call-update
  95.1 0.0 copy-start.7
  95.1 0.0 copy-start.8
  95.1 0.0 all-gather.9.cloned.1.call-start
  95.1 1.1 copy-done.1
  96.3 0.5 fusion.20
  96.7 0.7 copy-done.2
  97.5 1.2 fusion.19
  98.7 55.8 %reduce-scatter.2.cloned.1.call-done = f32[16,2048]{1,0:T(8,128)} async-done(((f32[256,2048]{1,0:T(8,128)}), f32[16,2048]{1,0:T(8,128)}) %reduce-scatter.2.cloned.1.call-update) | async-done | bytes 131088 | tf_op jit(solution)/shard_map/reduce_scatter | solution.py:57
  154.4 0.0 copy-done.7
  154.4 0.0 copy-done.8
  154.4 1.7 multiply_convert_fusion
  156.1 20.8 %all_gather.21 = bf16[256,1024]{1,0:T(8,128)(2,1)S(1)} all-gather(bf16[16,1024]{1,0:T(8,128)(2,1)S(1)} %get-tuple-element.26), channel_id=1, replica_groups=mesh['fs'=16,'tp'=2] {'fs'}, dimensions={0}, use_global_device_ids=true | all-gather | bytes 557056 | tf_op jit(solution)/shard_map/all_gather | solution.py:70
  176.9 18.9 %all_gather.20 = bf16[256,1024]{1,0:T(8,128)(2,1)S(1)} all-gather(bf16[16,1024]{1,0:T(8,128)(2,1)S(1)} %get-tuple-element.32), channel_id=1, replica_groups=mesh['fs'=16,'tp'=2] {'fs'}, dimensions={0}, use_global_device_ids=true | all-gather | bytes 557056 | tf_op jit(solution)/shard_map/all_gather | solution.py:69
  195.7 1.2 fusion.13
  197.0 0.0 copy-done.3
  197.0 1.0 fusion.5
  198.0 0.3 fusion.10
  198.3 1.0 fusion.6
  199.4 2.1 copy.22
  201.4 4.4 %all-reduce = (f32[]{:T(128)}, f32[]{:T(128)}) all-reduce(f32[]{:T(128)} %fusion.5, f32[]{:T(128)} %fusion.6), channel_id=1, replica_groups=mesh['fs'=16,'tp'=2] {'tp'}, use_global_device_ids=true, to_apply=%region_2.0 | all-reduce | flops 2 | bytes 16 | tf_op jit(solution)/shard_map/psum | solution.py:82
  206.5 0.0 copy-done.5
  206.5 2.4 fusion.16
  209.0 0.0 all-gather.9.cloned.1.call-update
  209.0 0.0 all-gather.11.cloned.1.call-start
  209.8 0.0 copy-done.6
  209.8 2.5 fusion.15
  212.3 0.0 all-gather.11.cloned.1.call-update
  212.3 2.0 copy.24
  214.3 0.0 copy-done.4
  214.3 1.0 copy.23
  215.3 46.8 %all-gather.9.cloned.1.call-done = bf16[2048,1024]{0,1:T(8,128)(2,1)} async-done(((bf16[128,1024]{0,1:T(8,128)(2,1)}), bf16[2048,1024]{0,1:T(8,128)(2,1)}) %all-gather.9.cloned.1.call-update) | async-done | bytes 4194320 | tf_op jit(solution)/shard_map/all_gather | solution.py:91
  262.1 6.4 %copy.25 = bf16[2048,1024]{1,0:T(8,128)(2,1)} copy(bf16[2048,1024]{0,1:T(8,128)(2,1)} %all-gather.9.cloned.1.call-done) | data formatting | bytes 8388608
  268.5 46.3 %all-gather.11.cloned.1.call-done = bf16[1024,2048]{1,0:T(8,128)(2,1)} async-done(((bf16[1024,128]{1,0:T(8,128)(2,1)}), bf16[1024,2048]{1,0:T(8,128)(2,1)}) %all-gather.11.cloned.1.call-update) | async-done | bytes 4194320 | tf_op jit(solution)/shard_map/all_gather | solution.py:92
  314.8 4.8 %copy.27 = bf16[1024,2048]{1,0:T(8,128)(2,1)} copy(bf16[1024,2048]{1,0:T(8,128)(2,1)} %all-gather.11.cloned.1.call-done) | data formatting | bytes 8388608
  (5 shorter events, 0.0 us)
Async XLA Ops:
  7.2 41.4 %copy-start = (bf16[512,2048]{1,0:T(8,128)(2,1)S(1)}, bf16[512,2048]{1,0:T(8,128)(2,1)}, u32[]{:S(2)}) copy-start(bf16[512,2048]{1,0:T(8,128)(2,1)} %param.15) | copy-start | bytes 6291460
  7.2 41.4 %all-gather.7.cloned.1.call-start = ((), (), s32[]{:S(2)}) async-start(), calls=%async_computation.2 | async-start | bytes 1114112 | tf_op jit(solution)/shard_map/all_gather | solution.py:36
  7.9 79.6 %all-gather.5.cloned.1.call-start = ((), (), s32[]{:S(2)}) async-start(), calls=%async_computation.1 | async-start | bytes 1114112 | tf_op jit(solution)/shard_map/all_gather | solution.py:35
  8.7 145.7 %reduce-scatter.2.cloned.1.call-start = ((), (), s32[]{:S(2)}) async-start(), calls=%async_computation.3 | async-start | bytes 2228224 | tf_op jit(solution)/shard_map/reduce_scatter | solution.py:57
  95.0 1.2 copy-start.1
  95.1 59.4 %copy-start.7 = (f32[16,1024]{1,0:T(8,128)S(1)}, f32[16,1024]{1,0:T(8,128)}, u32[]{:S(2)}) copy-start(f32[16,1024]{1,0:T(8,128)} %param.23) | copy-start | bytes 196612
  95.1 59.4 %copy-start.8 = (f32[16,1024]{1,0:T(8,128)S(1)}, f32[16,1024]{1,0:T(8,128)}, u32[]{:S(2)}) copy-start(f32[16,1024]{1,0:T(8,128)} %param.22) | copy-start | bytes 196612
  95.1 167.0 %all-gather.9.cloned.1.call-start = ((), (), s32[]{:S(2)}) async-start(), calls=%async_computation.4 | async-start | bytes 4456448 | tf_op jit(solution)/shard_map/all_gather | solution.py:91
  96.3 1.2 copy-start.2
  154.4 42.6 %copy-start.3 = (f32[256,256]{1,0:T(8,128)S(1)}, f32[256,256]{1,0:T(8,128)}, u32[]{:S(2)}) copy-start(f32[256,256]{1,0:T(8,128)} %fusion.19) | copy-start | bytes 786436
  198.0 8.5 %copy-start.5 = (bf16[128,256]{1,0:T(8,128)(2,1)S(1)}, bf16[128,256]{1,0:T(8,128)(2,1)}, u32[]{:S(2)}) copy-start(bf16[128,256]{1,0:T(8,128)(2,1)} %param.16) | copy-start | bytes 196612
  199.4 10.4 %copy-start.6 = (bf16[128,256]{1,0:T(8,128)(2,1)S(1)}, bf16[128,256]{1,0:T(8,128)(2,1)}, u32[]{:S(2)}) copy-start(bf16[128,256]{1,0:T(8,128)(2,1)} %param.17) | copy-start | bytes 196612
  209.0 5.3 %copy-start.4 = (f32[128,1024]{0,1:T(8,128)S(1)}, f32[128,1024]{0,1:T(8,128)}, u32[]{:S(2)}) copy-start(f32[128,1024]{0,1:T(8,128)} %get-tuple-element.35) | copy-start | bytes 1572868
  209.0 105.8 %all-gather.11.cloned.1.call-start = ((), (), s32[]{:S(2)}) async-start(), calls=%async_computation.5 | async-start | bytes 4456448 | tf_op jit(solution)/shard_map/all_gather | solution.py:92
Sparse Core Ops, SparseCore 0:
  10.2 38.3 all-gather.6
  50.7 36.8 all-gather.4
  95.2 59.1 reduce-scatter.1
  209.1 52.9 all-gather.8
  264.1 50.6 all-gather.10
where the time goes:
time: 330 us; the launch traced here: 326 us
  waiting for transfers between devices  226 us (68%)
  blocking collectives  44 us (13%)
  local copies, waits for them, and re-layouts  18.2 us (6%)
  matrix products  18 us (5%)
  between operations  15.3 us (5%)
  other arithmetic  4.42 us (1%)
    reduce_scatter x1, waiting for transfers between devices, body(): lax.psum_scatter(jnp.concatenate([term_value, term_output], axis=1), 'fs'...  55.8 us
    all_gather x1, waiting for transfers between devices, body(): lax.all_gather(half_value, 'fs', axis=0, tiled=True)  46.8 us
    all_gather x1, waiting for transfers between devices, body(): lax.all_gather(half_output, 'fs', axis=1, tiled=True)  46.3 us
    all_gather x1, waiting for transfers between devices, body(): lax.all_gather(factor_output, 'fs', axis=0, tiled=True)  39.8 us
    all_gather x1, waiting for transfers between devices, body(): lax.all_gather(factor_value, 'fs', axis=0, tiled=True)  35.9 us
    all_gather x1, blocking collectives, body(): lax.all_gather(direction_output, 'fs', axis=0, tiled=True)  20.8 us
    all_gather x1, blocking collectives, body(): lax.all_gather(direction_value, 'fs', axis=0, tiled=True)  18.9 us
    unnamed x23, local copies, waits for them, and re-layouts  18.2 us
  transfers between devices with their start and end apart: 5, of which 5 were waited for; matrix products, arithmetic and copies ran while one was open for 5% of the time, Pallas kernels for 0%

commit v1 on v0

--- a/solution.py
+++ b/solution.py
@@ -1,7 +1,13 @@
+import functools
+
 import jax
 import jax.numpy as jnp
 from jax import lax
+from jax.experimental import pallas as pl
+from jax.experimental.pallas import tpu as pltpu
 from jax.sharding import PartitionSpec as P
+
+CORES = 2
 
 D = 2048
 WIDTH = 2048
@@ -105,7 +111,404 @@
     )
 
 
+class Relay:
+    def __init__(self, place, block, send_sem, recv_sem):
+        self.z, self.x, self.core, self.depth, self.width = place
+        self.block, self.send_sem, self.recv_sem = block, send_sem, recv_sem
+        self.pending = []
+
+    def index(self, shift, x, core):
+        z = lax.rem(self.z + shift, self.depth)
+        return (z * self.width + x) * CORES + core
+
+    def copy(self, origin, target, slot):
+        return pltpu.make_async_remote_copy(
+            src_ref=self.block(origin),
+            dst_ref=self.block(origin),
+            send_sem=self.send_sem.at[slot],
+            recv_sem=self.recv_sem.at[origin],
+            device_id={"fs": target},
+            device_id_type=pl.DeviceIdType.MESH,
+        )
+
+    def send(self, origin, target):
+        copy = self.copy(origin, target, len(self.pending))
+        copy.start()
+        self.pending.append(copy)
+
+    def arrived(self, origin):
+        self.copy(origin, self.index(0, self.x, 1 - self.core), 0).wait_recv()
+
+    def over_x(self, origin):
+        self.send(origin, self.index(0, 1 - self.x, self.core))
+
+    def over_core(self, origin):
+        self.send(origin, self.index(0, self.x, 1 - self.core))
+
+    def order(self):
+        shifts = []
+        for hop in range(1, self.depth // 2 + 1):
+            for shift in (hop, self.depth - hop):
+                if shift not in shifts:
+                    shifts.append(shift)
+        return shifts
+
+    def begin(self):
+        own = self.index(0, self.x, self.core)
+        for shift in self.order():
+            self.send(own, self.index(shift, self.x, self.core))
+        self.over_x(own)
+        self.over_core(own)
+
+    def along_z(self, shift):
+        origin = self.index(shift, self.x, self.core)
+        self.arrived(origin)
+        self.over_x(origin)
+        self.over_core(origin)
+
+    def across(self, shift):
+        origin = self.index(shift, 1 - self.x, self.core)
+        self.arrived(origin)
+        self.over_core(origin)
+
+    def middle(self):
+        lagged = [0]
+        for shift in self.order():
+            yield functools.partial(self.along_z, shift)
+            lagged.append(shift)
+            if len(lagged) > 1:
+                yield functools.partial(self.across, lagged.pop(0))
+        for shift in lagged:
+            yield functools.partial(self.across, shift)
+
+    def finish(self):
+        for shift in [0] + self.order():
+            for x in (self.x, 1 - self.x):
+                self.arrived(self.index(shift, x, 1 - self.core))
+        for copy in self.pending:
+            copy.wait_send()
+
+
+def fused(
+    fs_size,
+    tp_size,
+    input_hbm,
+    value_hbm,
+    gated_hbm,
+    layer_hbm,
+    factor_value_hbm,
+    factor_output_hbm,
+    weight_value_ref,
+    weight_output_ref,
+    first_value_ref,
+    second_value_ref,
+    first_output_ref,
+    second_output_ref,
+    step_value_ref,
+    step_output_ref,
+    next_weight_value_ref,
+    next_weight_output_ref,
+    next_first_value_ref,
+    next_second_value_ref,
+    next_first_output_ref,
+    next_second_output_ref,
+    copy_value_ref,
+    copy_output_ref,
+    stream,
+    cotan,
+    factors,
+    projected,
+    terms,
+    paired,
+    outgoing,
+    incoming,
+    directions,
+    totals,
+    load_sem,
+    pair_send,
+    pair_recv,
+    sum_send,
+    sum_recv,
+    total_send,
+    total_recv,
+    relay_send,
+    relay_recv,
+):
+    fs, tp = lax.axis_index("fs"), lax.axis_index("tp")
+    width = tp_size
+    chips = fs_size // CORES
+    depth = chips // width
+    core, chip = lax.rem(fs, CORES), fs // CORES
+    x, z = lax.rem(chip, width), chip // width
+    place = (z, x, core, depth, width)
+    partner = chip * CORES + 1 - core
+    mesh_id = pl.DeviceIdType.MESH
+    rows = factor_value_hbm.shape[0]
+    tokens = input_hbm.shape[0]
+    cols = value_hbm.shape[1]
+    ranks = first_value_ref.shape[0]
+    everyone = [(a, b) for a in range(fs_size) for b in range(tp_size)][1:]
+
+    own_rows = pl.ds(pl.multiple_of(fs * rows, rows), rows)
+    loads = [
+        pltpu.make_async_copy(source, target, load_sem.at[slot])
+        for slot, (source, target) in enumerate(
+            (
+                (factor_value_hbm, factors.at[0, own_rows]),
+                (factor_output_hbm, factors.at[1, own_rows]),
+                (input_hbm, stream.at[0]),
+                (layer_hbm, stream.at[1]),
+                (value_hbm, cotan.at[0]),
+                (gated_hbm, cotan.at[1]),
+            )
+        )
+    ]
+    for load in loads:
+        load.start()
+
+    barrier = pltpu.get_barrier_semaphore()
+    for a, b in everyone:
+        pl.semaphore_signal(
+            barrier,
+            inc=1,
+            device_id={"fs": lax.rem(fs + a, fs_size), "tp": lax.rem(tp + b, tp_size)},
+            device_id_type=mesh_id,
+        )
+    loads[0].wait()
+    loads[1].wait()
+    pl.semaphore_wait(barrier, len(everyone))
+
+    def row_block(ref, size, lead=False):
+        def block(origin):
+            span = pl.ds(pl.multiple_of(origin * size, size), size)
+            return ref.at[:, span] if lead else ref.at[span]
+
+        return block
+
+    def column_block(origin):
+        return copy_output_ref.at[:, pl.ds(pl.multiple_of(origin * rows, rows), rows)]
+
+    relays = [
+        Relay(place, block, relay_send.at[slot], relay_recv.at[slot])
+        for slot, block in enumerate(
+            (
+                row_block(factors, rows, True),
+                row_block(directions, ranks),
+                row_block(copy_value_ref, rows),
+                column_block,
+            )
+        )
+    ]
+
+    relays[0].begin()
+    for step in relays[0].middle():
+        step()
+    relays[0].finish()
+    for load in loads[2:]:
+        load.wait()
+
+    tile = 128
+    for kind in range(2):
+
+        @pl.loop(0, tokens // tile)
+        def _(step, kind=kind):
+            span = pl.ds(pl.multiple_of(step * tile, tile), tile)
+            projected[kind, span] = jnp.dot(
+                stream[kind, span], factors[kind], preferred_element_type=jnp.float32
+            ).astype(jnp.bfloat16)
+
+    width_tile = 256
+    for kind in range(2):
+
+        @pl.loop(0, cols // width_tile)
+        def _(step, kind=kind):
+            span = pl.ds(pl.multiple_of(step * width_tile, width_tile), width_tile)
+            term = lax.dot_general(
+                projected[kind],
+                cotan[kind, :, span],
+                (((0,), (0,)), ((), ())),
+                preferred_element_type=jnp.float32,
+            )
+            target = pl.ds(pl.multiple_of(kind * cols + step * width_tile, width_tile), width_tile)
+            terms[:, :, :, target] = term.reshape(chips, CORES, ranks, width_tile)
+
+    pairs = []
+    for shift in list(range(1, chips)) + [0]:
+        c = lax.rem(chip + shift, chips)
+        copy = pltpu.make_async_remote_copy(
+            src_ref=terms.at[c, 1 - core],
+            dst_ref=paired.at[c],
+            send_sem=pair_send.at[shift],
+            recv_sem=pair_recv.at[c],
+            device_id={"fs": partner},
+            device_id_type=mesh_id,
+        )
+        copy.start()
+        pairs.append(copy)
+    sums = []
+    for shift in range(1, chips):
+        c = lax.rem(chip + shift, chips)
+        pairs[shift - 1].wait_recv()
+        outgoing[c] = (terms[c, core] + paired[c]).astype(jnp.bfloat16)
+        copy = pltpu.make_async_remote_copy(
+            src_ref=outgoing.at[c],
+            dst_ref=incoming.at[chip],
+            send_sem=sum_send.at[shift],
+            recv_sem=sum_recv.at[chip],
+            device_id={"fs": c * CORES + core},
+            device_id_type=mesh_id,
+        )
+        copy.start()
+        sums.append(copy)
+    pairs[-1].wait_recv()
+    low = terms[chip, core] + paired[chip]
+    for shift in range(1, chips):
+        c = lax.rem(chip + chips - shift, chips)
+        pltpu.make_async_remote_copy(
+            src_ref=outgoing.at[c],
+            dst_ref=incoming.at[c],
+            send_sem=sum_send.at[shift],
+            recv_sem=sum_recv.at[c],
+            device_id={"fs": c * CORES + core},
+            device_id_type=mesh_id,
+        ).wait_recv()
+        low = low + incoming[c].astype(jnp.float32)
+
+    own_ranks = pl.ds(pl.multiple_of(fs * ranks, ranks), ranks)
+    moments = (
+        (first_value_ref, second_value_ref, next_first_value_ref, next_second_value_ref),
+        (first_output_ref, second_output_ref, next_first_output_ref, next_second_output_ref),
+    )
+    for kind, (first_ref, second_ref, next_first_ref, next_second_ref) in enumerate(moments):
+        part = low[:, kind * cols : (kind + 1) * cols]
+        next_first = 0.9 * first_ref[...] + 0.1 * part
+        next_second = 0.95 * second_ref[...] + 0.05 * part * part
+        next_first_ref[...] = next_first
+        next_second_ref[...] = next_second
+        directions[own_ranks, kind * cols : (kind + 1) * cols] = (
+            next_first * lax.rsqrt(next_second)
+        ).astype(jnp.bfloat16)
+    relays[1].begin()
+    for step in relays[1].middle():
+        step()
+    relays[1].finish()
+
+    me = fs * tp_size + tp
+    for kind, step_ref in enumerate((step_value_ref, step_output_ref)):
+        square = jnp.zeros((8, 128), jnp.float32)
+        for start in range(0, cols, width_tile):
+            update = jnp.dot(
+                factors[kind, own_rows],
+                directions[:, kind * cols + start : kind * cols + start + width_tile],
+                preferred_element_type=jnp.float32,
+            )
+            if kind == 0:
+                step_ref[:, start : start + width_tile] = update
+            else:
+                step_ref[start : start + width_tile, :] = update.T
+            fold = jnp.sum((update * update).reshape(rows // 8, 8, width_tile), axis=0)
+            for lane in range(0, width_tile, 128):
+                square = square + fold[:, lane : lane + 128]
+        totals[me, kind] = square
+    shares = []
+    for slot, (a, b) in enumerate(everyone):
+        copy = pltpu.make_async_remote_copy(
+            src_ref=totals.at[me],
+            dst_ref=totals.at[me],
+            send_sem=total_send.at[slot],
+            recv_sem=total_recv.at[me],
+            device_id={"fs": lax.rem(fs + a, fs_size), "tp": lax.rem(tp + b, tp_size)},
+            device_id_type=mesh_id,
+        )
+        copy.start()
+        shares.append(copy)
+    for a, b in everyone:
+        other_fs, other_tp = lax.rem(fs + a, fs_size), lax.rem(tp + b, tp_size)
+        other = other_fs * tp_size + other_tp
+        pltpu.make_async_remote_copy(
+            src_ref=totals.at[other],
+            dst_ref=totals.at[other],
+            send_sem=total_send.at[0],
+            recv_sem=total_recv.at[other],
+            device_id={"fs": other_fs, "tp": other_tp},
+            device_id_type=mesh_id,
+        ).wait_recv()
+    entries = rows * fs_size * cols * tp_size
+    scales = []
+    for kind in range(2):
+        total = jnp.sum(jnp.sum(totals[:, kind], axis=0), keepdims=True)
+        scales.append(lax.rsqrt(total / entries + 1e-06))
+
+    step_value = step_value_ref[...] * scales[0]
+    next_weight = weight_value_ref[...] - 0.02 * step_value
+    step_value_ref[...] = step_value
+    next_weight_value_ref[...] = next_weight
+    copy_value_ref[own_rows, :] = next_weight.astype(jnp.bfloat16)
+    relays[2].begin()
+    step_output = step_output_ref[...] * scales[1]
+    next_weight = weight_output_ref[...] - 0.02 * step_output
+    step_output_ref[...] = step_output
+    next_weight_output_ref[...] = next_weight
+    copy_output_ref[:, own_rows] = next_weight.astype(jnp.bfloat16)
+    relays[3].begin()
+    for first, second in zip(relays[2].middle(), relays[3].middle()):
+        first()
+        second()
+    relays[2].finish()
+    relays[3].finish()
+    for copy in pairs + sums + shares:
+        copy.wait_send()
+
+
+def fused_body(fs_size, tp_size, *args):
+    tokens, model = args[0].shape
+    cols = args[1].shape[1]
+    rows, rank = args[4].shape
+    ranks = args[8].shape[0]
+    chips = fs_size // CORES
+    f32, bf16 = jnp.float32, jnp.bfloat16
+    vmem, anywhere = pl.BlockSpec(memory_space=pltpu.VMEM), pl.BlockSpec(memory_space=pl.ANY)
+    shape = jax.ShapeDtypeStruct
+    hops = chips // tp_size - 1 + chips // tp_size + chips
+    dma = pltpu.SemaphoreType.DMA
+    return pl.pallas_call(
+        functools.partial(fused, fs_size, tp_size),
+        out_shape=(
+            [shape((rows, cols), f32), shape((cols, rows), f32)] * 2
+            + [shape((ranks, cols), f32)] * 4
+            + [shape((model, cols), bf16), shape((cols, model), bf16)]
+        ),
+        in_specs=[anywhere] * 6 + [vmem] * 6,
+        out_specs=[vmem] * 10,
+        scratch_shapes=[
+            pltpu.VMEM((2, tokens, model), bf16),
+            pltpu.VMEM((2, tokens, cols), bf16),
+            pltpu.VMEM((2, model, rank), bf16),
+            pltpu.VMEM((2, tokens, rank), bf16),
+            pltpu.VMEM((chips, CORES, ranks, 2 * cols), f32),
+            pltpu.VMEM((chips, ranks, 2 * cols), f32),
+            pltpu.VMEM((chips, ranks, 2 * cols), bf16),
+            pltpu.VMEM((chips, ranks, 2 * cols), bf16),
+            pltpu.VMEM((rank, 2 * cols), bf16),
+            pltpu.VMEM((fs_size * tp_size, 2, 8, 128), f32),
+            dma((6,)),
+            dma((chips,)),
+            dma((chips,)),
+            dma((chips,)),
+            dma((chips,)),
+            dma((fs_size * tp_size,)),
+            dma((fs_size * tp_size,)),
+            dma((4, hops)),
+            dma((4, fs_size)),
+        ],
+        compiler_params=pltpu.CompilerParams(
+            collective_id=0, has_side_effects=True, vmem_limit_bytes=60 * 1024 * 1024
+        ),
+    )(*args)
+
+
 def solution(mesh):
+    fs_size, tp_size = mesh.shape["fs"], mesh.shape["tp"]
     placed = (
         P("fs", None),
         P("fs", "tp"),
@@ -120,8 +523,10 @@
         P("fs", "tp"),
         P("fs", "tp"),
     )
+    chips = fs_size // CORES
+    tiled = tp_size == 2 and fs_size == 16 and chips % tp_size == 0
     return jax.shard_map(
-        body,
+        functools.partial(fused_body, fs_size, tp_size) if tiled else body,
         mesh=mesh,
         in_specs=placed,
         out_specs=(

time: 330 us -> 163 us (0.49); the launches traced: 326 us -> 163 us
  waiting for transfers between devices: 226 us -> 0 us
  Pallas kernels: 0 us -> 144 us
  blocking collectives: 44 us -> 0 us
  matrix products: 18 us -> 0 us
  between operations: 15.3 us -> 0.69 us
  other arithmetic: 4.42 us -> 0 us
    all_gather x4 -> x0, waiting for transfers between devices: 169 us -> none  [the longest x1 46.8 us: body(): lax.all_gather(half_value, 'fs', axis=0, tiled=True)]
    pallas_call x0 -> x1, Pallas kernels: none -> 144 us  [fused_body(): pl.pallas_call(functools.partial(fused, fs_size, tp_size), out_shape=[sha...]
    reduce_scatter x1 -> x0, waiting for transfers between devices: 55.8 us -> none  [body(): lax.psum_scatter(jnp.concatenate([term_value, term_output], axis=1), 'fs'...]
    all_gather x2 -> x0, blocking collectives: 39.6 us -> none  [the longest x1 20.8 us: body(): lax.all_gather(direction_output, 'fs', axis=0, tiled=True)]
    dot_general x10 -> x0, matrix products: 18 us -> none  [the longest x1 4.73 us: body(): lax.dot_general(span_input, value_cotangent, inner, preferred_element_typ...]
    psum x1 -> x0, blocking collectives: 4.39 us -> none  [body(): total_value, total_output = lax.psum((square_value, square_output), 'tp')]
    unnamed x23 -> x18, local copies, waits for them, and re-layouts: 18.2 us -> 17.6 us
  transfers between devices with their start and end apart: 5 -> 0, of which waited for: 5 -> 0; matrix products, arithmetic and copies ran while one was open for 5% -> 0% of each run, Pallas kernels for 0% -> 0%
where the time goes in v1:
time: 163 us
  Pallas kernels  144 us (88%)
  local copies, waits for them, and re-layouts  17.6 us (11%)
    pallas_call x1, Pallas kernels, fused_body(): pl.pallas_call(functools.partial(fused, fs_size, tp_size), out_shape=[sha...  144 us
    unnamed x18, local copies, waits for them, and re-layouts  17.6 us

profile of v1, /device:TPU:9, one launch (start us, length us, event | category | flops | bytes accessed | tf_op | source)
XLA Modules:
  0.0 162.8 jit_solution(3034368806846341684)
XLA Ops:
  0.6 144.5 %shard_map.195 = (f32[128,1024]{1,0:T(8,128)}, f32[1024,128]{1,0:T(8,128)}, f32[128,1024]{1,0:T(8,128)}, f32[1024,128]{1,0:T(8,128)}, f32[16,1024]{1,0:T(8,128)}...) custom-call(bf16[512,2048]{1,0:T(8,128)(2,1)} %input_hbm.1, ...), custom_call_target="tpu_custom_call" | custom-call | tf_op jit(solution)/shard_map/pallas_call | solution.py:474
  145.1 0.0 copy-start.3
  145.1 0.0 copy-start.2
  145.2 0.0 copy-start.1
  145.2 2.0 %copy.32 = f32[128,1024]{1,0:T(8,128)} copy(f32[128,1024]{1,0:T(8,128)} %get-tuple-element.20) | data formatting | bytes 1048576
  147.2 1.9 %copy.33 = f32[1024,128]{1,0:T(8,128)} copy(f32[1024,128]{1,0:T(8,128)} %get-tuple-element.21) | data formatting | bytes 1048576
  149.1 1.9 %copy.34 = f32[128,1024]{1,0:T(8,128)} copy(f32[128,1024]{1,0:T(8,128)} %get-tuple-element.22) | data formatting | bytes 1048576
  151.0 1.9 %copy.35 = f32[1024,128]{1,0:T(8,128)} copy(f32[1024,128]{1,0:T(8,128)} %get-tuple-element.23) | data formatting | bytes 1048576
  152.8 1.5 copy.36
  154.3 1.5 copy.37
  155.8 0.0 copy-done.3
  155.8 0.6 copy.38
  156.4 0.0 copy-done.2
  156.4 0.6 copy.39
  157.0 0.0 copy-done.1
  157.0 0.0 copy-start
  157.0 2.1 %copy.40 = bf16[2048,1024]{1,0:T(8,128)(2,1)} copy(bf16[2048,1024]{1,0:T(8,128)(2,1)S(1)} %copy-done.1) | data formatting | bytes 8388608
  159.2 1.6 copy-done
  160.7 2.0 %copy.41 = bf16[1024,2048]{1,0:T(8,128)(2,1)} copy(bf16[1024,2048]{1,0:T(8,128)(2,1)S(1)} %copy-done) | data formatting | bytes 8388608
Async XLA Ops:
  145.1 10.6 %copy-start.3 = (f32[16,1024]{1,0:T(8,128)S(1)}, f32[16,1024]{1,0:T(8,128)}, u32[]{:S(2)}) copy-start(f32[16,1024]{1,0:T(8,128)} %get-tuple-element.26) | copy-start | bytes 196612
  145.1 11.3 %copy-start.2 = (f32[16,1024]{1,0:T(8,128)S(1)}, f32[16,1024]{1,0:T(8,128)}, u32[]{:S(2)}) copy-start(f32[16,1024]{1,0:T(8,128)} %get-tuple-element.27) | copy-start | bytes 196612
  145.2 11.9 %copy-start.1 = (bf16[2048,1024]{1,0:T(8,128)(2,1)S(1)}, bf16[2048,1024]{1,0:T(8,128)(2,1)}, u32[]{:S(2)}) copy-start(bf16[2048,1024]{1,0:T(8,128)(2,1)} %get-tuple-element.28) | copy-start | bytes 12582916
  157.0 3.7 %copy-start = (bf16[1024,2048]{1,0:T(8,128)(2,1)S(1)}, bf16[1024,2048]{1,0:T(8,128)(2,1)}, u32[]{:S(2)}) copy-start(bf16[1024,2048]{1,0:T(8,128)(2,1)} %get-tuple-element.29) | copy-start | bytes 12582916

commit v2 on v1

--- a/solution.py
+++ b/solution.py
@@ -189,6 +189,10 @@
             copy.wait_send()
 
 
+def next_moments(first, second, low):
+    return 0.9 * first + 0.1 * low, 0.95 * second + 0.05 * low * low
+
+
 def fused(
     fs_size,
     tp_size,
@@ -204,25 +208,19 @@
     second_value_ref,
     first_output_ref,
     second_output_ref,
-    step_value_ref,
-    step_output_ref,
-    next_weight_value_ref,
-    next_weight_output_ref,
-    next_first_value_ref,
-    next_second_value_ref,
-    next_first_output_ref,
-    next_second_output_ref,
-    copy_value_ref,
-    copy_output_ref,
+    low_ref,
+    directions,
+    factors,
+    scale_ref,
+    wide_value_ref,
+    wide_output_ref,
     stream,
     cotan,
-    factors,
     projected,
     terms,
     paired,
     outgoing,
     incoming,
-    directions,
     totals,
     load_sem,
     pair_send,
@@ -285,24 +283,41 @@
 
         return block
 
-    def column_block(origin):
-        return copy_output_ref.at[:, pl.ds(pl.multiple_of(origin * rows, rows), rows)]
-
+    half = cols // 2
+
+    def rows_part(part):
+        def block(origin):
+            span = pl.ds(pl.multiple_of(origin * rows, rows), rows)
+            return wide_value_ref.at[span, part * half : (part + 1) * half]
+
+        return block
+
+    def columns_part(part):
+        def block(origin):
+            span = pl.ds(pl.multiple_of(origin * rows, rows), rows)
+            return wide_output_ref.at[part * half : (part + 1) * half, span]
+
+        return block
+
+    gathers = (
+        row_block(factors, rows, True),
+        row_block(directions, ranks),
+        rows_part(0),
+        rows_part(1),
+        columns_part(0),
+        columns_part(1),
+    )
     relays = [
         Relay(place, block, relay_send.at[slot], relay_recv.at[slot])
-        for slot, block in enumerate(
-            (
-                row_block(factors, rows, True),
-                row_block(directions, ranks),
-                row_block(copy_value_ref, rows),
-                column_block,
-            )
-        )
+        for slot, block in enumerate(gathers)
     ]
 
     relays[0].begin()
+    wide_value_ref[own_rows, :] = weight_value_ref[...].astype(jnp.bfloat16)
+    wide_output_ref[:, own_rows] = weight_output_ref[...].astype(jnp.bfloat16)
     for step in relays[0].middle():
         step()
+    relays[2].begin()
     relays[0].finish()
     for load in loads[2:]:
         load.wait()
@@ -316,6 +331,9 @@
             projected[kind, span] = jnp.dot(
                 stream[kind, span], factors[kind], preferred_element_type=jnp.float32
             ).astype(jnp.bfloat16)
+
+    for step in relays[2].middle():
+        step()
 
     width_tile = 256
     for kind in range(2):
@@ -360,6 +378,7 @@
         )
         copy.start()
         sums.append(copy)
+    relays[3].begin()
     pairs[-1].wait_recv()
     low = terms[chip, core] + paired[chip]
     for shift in range(1, chips):
@@ -375,26 +394,24 @@
         low = low + incoming[c].astype(jnp.float32)
 
     own_ranks = pl.ds(pl.multiple_of(fs * ranks, ranks), ranks)
-    moments = (
-        (first_value_ref, second_value_ref, next_first_value_ref, next_second_value_ref),
-        (first_output_ref, second_output_ref, next_first_output_ref, next_second_output_ref),
-    )
-    for kind, (first_ref, second_ref, next_first_ref, next_second_ref) in enumerate(moments):
+    low_ref[...] = low
+    moments = ((first_value_ref, second_value_ref), (first_output_ref, second_output_ref))
+    for kind, (first_ref, second_ref) in enumerate(moments):
         part = low[:, kind * cols : (kind + 1) * cols]
-        next_first = 0.9 * first_ref[...] + 0.1 * part
-        next_second = 0.95 * second_ref[...] + 0.05 * part * part
-        next_first_ref[...] = next_first
-        next_second_ref[...] = next_second
+        next_first, next_second = next_moments(first_ref[...], second_ref[...], part)
         directions[own_ranks, kind * cols : (kind + 1) * cols] = (
             next_first * lax.rsqrt(next_second)
         ).astype(jnp.bfloat16)
     relays[1].begin()
-    for step in relays[1].middle():
-        step()
+    for first, second in zip(relays[1].middle(), relays[3].middle()):
+        first()
+        second()
+    relays[4].begin()
+    relays[5].begin()
     relays[1].finish()
 
     me = fs * tp_size + tp
-    for kind, step_ref in enumerate((step_value_ref, step_output_ref)):
+    for kind in range(2):
         square = jnp.zeros((8, 128), jnp.float32)
         for start in range(0, cols, width_tile):
             update = jnp.dot(
@@ -402,10 +419,6 @@
                 directions[:, kind * cols + start : kind * cols + start + width_tile],
                 preferred_element_type=jnp.float32,
             )
-            if kind == 0:
-                step_ref[:, start : start + width_tile] = update
-            else:
-                step_ref[start : start + width_tile, :] = update.T
             fold = jnp.sum((update * update).reshape(rows // 8, 8, width_tile), axis=0)
             for lane in range(0, width_tile, 128):
                 square = square + fold[:, lane : lane + 128]
@@ -422,6 +435,9 @@
         )
         copy.start()
         shares.append(copy)
+    for first, second in zip(relays[4].middle(), relays[5].middle()):
+        first()
+        second()
     for a, b in everyone:
         other_fs, other_tp = lax.rem(fs + a, fs_size), lax.rem(tp + b, tp_size)
         other = other_fs * tp_size + other_tp
@@ -434,30 +450,77 @@
             device_id_type=mesh_id,
         ).wait_recv()
     entries = rows * fs_size * cols * tp_size
-    scales = []
     for kind in range(2):
         total = jnp.sum(jnp.sum(totals[:, kind], axis=0), keepdims=True)
-        scales.append(lax.rsqrt(total / entries + 1e-06))
-
-    step_value = step_value_ref[...] * scales[0]
-    next_weight = weight_value_ref[...] - 0.02 * step_value
-    step_value_ref[...] = step_value
-    next_weight_value_ref[...] = next_weight
-    copy_value_ref[own_rows, :] = next_weight.astype(jnp.bfloat16)
-    relays[2].begin()
-    step_output = step_output_ref[...] * scales[1]
-    next_weight = weight_output_ref[...] - 0.02 * step_output
-    step_output_ref[...] = step_output
-    next_weight_output_ref[...] = next_weight
-    copy_output_ref[:, own_rows] = next_weight.astype(jnp.bfloat16)
-    relays[3].begin()
-    for first, second in zip(relays[2].middle(), relays[3].middle()):
-        first()
-        second()
-    relays[2].finish()
-    relays[3].finish()
+        scale = lax.rsqrt(total / entries + 1e-06)
+        scale_ref[kind] = jnp.broadcast_to(scale, scale_ref.shape[1:])
+    for relay in relays[2:]:
+        relay.finish()
     for copy in pairs + sums + shares:
         copy.wait_send()
+
+
+def apply(
+    low_ref,
+    directions,
+    factors,
+    scale_ref,
+    wide_value_ref,
+    wide_output_ref,
+    factor_value_ref,
+    factor_output_ref,
+    weight_value_ref,
+    weight_output_ref,
+    first_value_ref,
+    second_value_ref,
+    first_output_ref,
+    second_output_ref,
+    step_value_ref,
+    step_output_ref,
+    next_weight_value_ref,
+    next_weight_output_ref,
+    next_first_value_ref,
+    next_second_value_ref,
+    next_first_output_ref,
+    next_second_output_ref,
+    copy_value_ref,
+    copy_output_ref,
+    turned,
+):
+    cols = weight_value_ref.shape[1]
+    scale_value, scale_output = scale_ref[0, :1, :1], scale_ref[1, :1, :1]
+    last = (((1,), (1,)), ((), ()))
+
+    def update_value(factor):
+        return jnp.dot(factor, directions[:, :cols], preferred_element_type=jnp.float32)
+
+    def update_output(factor):
+        return lax.dot_general(turned[...], factor, last, preferred_element_type=jnp.float32)
+
+    @pl.when(pl.program_id(0) == 0)
+    def _():
+        turned[...] = directions[:, cols:].astype(jnp.float32).T.astype(jnp.bfloat16)
+        moments = (
+            (first_value_ref, second_value_ref, next_first_value_ref, next_second_value_ref),
+            (first_output_ref, second_output_ref, next_first_output_ref, next_second_output_ref),
+        )
+        for kind, (first_ref, second_ref, next_first_ref, next_second_ref) in enumerate(moments):
+            next_first_ref[...], next_second_ref[...] = next_moments(
+                first_ref[...], second_ref[...], low_ref[:, kind * cols : (kind + 1) * cols]
+            )
+        step_value = update_value(factor_value_ref[...]) * scale_value
+        step_value_ref[...] = step_value
+        next_weight_value_ref[...] = weight_value_ref[...] - 0.02 * step_value
+        step_output = update_output(factor_output_ref[...]) * scale_output
+        step_output_ref[...] = step_output
+        next_weight_output_ref[...] = weight_output_ref[...] - 0.02 * step_output
+
+    copy_value_ref[...] = (
+        wide_value_ref[...].astype(jnp.float32) - update_value(factors[0]) * (0.02 * scale_value)
+    ).astype(jnp.bfloat16)
+    copy_output_ref[...] = (
+        wide_output_ref[...].astype(jnp.float32) - update_output(factors[1]) * (0.02 * scale_output)
+    ).astype(jnp.bfloat16)
 
 
 def fused_body(fs_size, tp_size, *args):
@@ -471,25 +534,26 @@
     shape = jax.ShapeDtypeStruct
     hops = chips // tp_size - 1 + chips // tp_size + chips
     dma = pltpu.SemaphoreType.DMA
-    return pl.pallas_call(
+    gathered = pl.pallas_call(
         functools.partial(fused, fs_size, tp_size),
-        out_shape=(
-            [shape((rows, cols), f32), shape((cols, rows), f32)] * 2
-            + [shape((ranks, cols), f32)] * 4
-            + [shape((model, cols), bf16), shape((cols, model), bf16)]
-        ),
+        out_shape=[
+            shape((ranks, 2 * cols), f32),
+            shape((rank, 2 * cols), bf16),
+            shape((2, model, rank), bf16),
+            shape((2, 8, 128), f32),
+            shape((model, cols), bf16),
+            shape((cols, model), bf16),
+        ],
         in_specs=[anywhere] * 6 + [vmem] * 6,
-        out_specs=[vmem] * 10,
+        out_specs=[vmem] * 6,
         scratch_shapes=[
             pltpu.VMEM((2, tokens, model), bf16),
             pltpu.VMEM((2, tokens, cols), bf16),
-            pltpu.VMEM((2, model, rank), bf16),
             pltpu.VMEM((2, tokens, rank), bf16),
             pltpu.VMEM((chips, CORES, ranks, 2 * cols), f32),
             pltpu.VMEM((chips, ranks, 2 * cols), f32),
             pltpu.VMEM((chips, ranks, 2 * cols), bf16),
             pltpu.VMEM((chips, ranks, 2 * cols), bf16),
-            pltpu.VMEM((rank, 2 * cols), bf16),
             pltpu.VMEM((fs_size * tp_size, 2, 8, 128), f32),
             dma((6,)),
             dma((chips,)),
@@ -498,13 +562,40 @@
             dma((chips,)),
             dma((fs_size * tp_size,)),
             dma((fs_size * tp_size,)),
-            dma((4, hops)),
-            dma((4, fs_size)),
+            dma((6, hops)),
+            dma((6, fs_size)),
         ],
         compiler_params=pltpu.CompilerParams(
             collective_id=0, has_side_effects=True, vmem_limit_bytes=60 * 1024 * 1024
         ),
     )(*args)
+
+    tile = 2 * rows
+
+    def whole(array):
+        return pl.BlockSpec(array.shape, lambda i: (0,) * len(array.shape))
+
+    by_rows = pl.BlockSpec((tile, cols), lambda i: (i, 0))
+    by_columns = pl.BlockSpec((cols, tile), lambda i: (0, i))
+    own = [shape((rows, cols), f32), shape((cols, rows), f32)] * 2 + [shape((ranks, cols), f32)] * 4
+    low, directions, factors, scales = gathered[:4]
+    return pl.pallas_call(
+        apply,
+        grid=(model // tile,),
+        out_shape=own + [shape((model, cols), bf16), shape((cols, model), bf16)],
+        in_specs=[
+            whole(low),
+            whole(directions),
+            pl.BlockSpec((2, tile, rank), lambda i: (0, i, 0)),
+            whole(scales),
+            by_rows,
+            by_columns,
+        ]
+        + [whole(array) for array in args[4:]],
+        out_specs=[whole(array) for array in own] + [by_rows, by_columns],
+        scratch_shapes=[pltpu.VMEM((cols, rank), bf16)],
+        compiler_params=pltpu.CompilerParams(vmem_limit_bytes=60 * 1024 * 1024),
+    )(*gathered, *args[4:])
 
 
 def solution(mesh):

time: 163 us -> 143 us (0.88)
  local copies, waits for them, and re-layouts: 17.6 us -> 0 us
  Pallas kernels: 144 us -> 142 us
    unnamed x18 -> x0, local copies, waits for them, and re-layouts: 17.6 us -> none
    pallas_call x1, Pallas kernels: 144 us -> 130 us  [fused_body(): pl.pallas_call(functools.partial(fused, fs_size, tp_size), out_shape=[sha...]
    pallas_call x0 -> x1, Pallas kernels: none -> 12.1 us  [fused_body(): pl.pallas_call(apply, grid=(model // tile,), out_shape=own + [shape((mode...]
where the time goes in v2:
time: 143 us; the launch traced here: 142 us
  Pallas kernels  142 us (99%)
    pallas_call x1, Pallas kernels, fused_body(): pl.pallas_call(functools.partial(fused, fs_size, tp_size), out_shape=[sha...  130 us
    pallas_call x1, Pallas kernels, fused_body(): pl.pallas_call(apply, grid=(model // tile,), out_shape=own + [shape((mode...  12.1 us

profile of v2, /device:TPU:9, one launch (start us, length us, event | category | flops | bytes accessed | tf_op | source)
XLA Modules:
  0.0 142.5 jit_solution(11147982520141527931)
XLA Ops:
  0.6 129.7 %shard_map.195 = (f32[16,2048]{1,0:T(8,128)}, bf16[256,2048]{1,0:T(8,128)(2,1)}, bf16[2,2048,256]{2,1,0:T(8,128)(2,1)}, f32[2,8,128]{2,1,0:T(8,128)}, bf16[2048,...) custom-call(bf16[512,2048]{1,0:T(8,128)(2,1)} %input_hbm.1, bf16[512,1024]{1,0:T(8,128)(2,1)} %value_hbm.1, ...), custom_call_target="tpu_custom_call" | custom-call | tf_op jit(solution)/shard_map/pallas_call | solution.py:537
  130.4 12.1 %shard_map.196 = (f32[128,1024]{1,0:T(8,128)}, f32[1024,128]{1,0:T(8,128)}, f32[128,1024]{1,0:T(8,128)}, f32[1024,128]{1,0:T(8,128)}, f32[16,1024]{1,0:T(8,128)}...) custom-call(f32[16,2048]{1,0:T(8,128)} %get-tuple-element.16.low_ref, ...), custom_call_target="tpu_custom_call" | custom-call | tf_op jit(solution)/shard_map/pallas_call | solution.py:582

commit v3 on v2

--- a/solution.py
+++ b/solution.py
@@ -332,9 +332,6 @@
                 stream[kind, span], factors[kind], preferred_element_type=jnp.float32
             ).astype(jnp.bfloat16)
 
-    for step in relays[2].middle():
-        step()
-
     width_tile = 256
     for kind in range(2):
 
@@ -378,6 +375,8 @@
         )
         copy.start()
         sums.append(copy)
+    for step in relays[2].middle():
+        step()
     relays[3].begin()
     pairs[-1].wait_recv()
     low = terms[chip, core] + paired[chip]

time: 143 us -> 130 us (0.909)
  Pallas kernels: 142 us -> 129 us
    pallas_call x1, Pallas kernels: 130 us -> 117 us  [fused_body(): pl.pallas_call(functools.partial(fused, fs_size, tp_size), out_shape=[sha...]
where the time goes in v3:
time: 130 us
  Pallas kernels  129 us (99%)
    pallas_call x1, Pallas kernels, fused_body(): pl.pallas_call(functools.partial(fused, fs_size, tp_size), out_shape=[sha...  117 us
    pallas_call x1, Pallas kernels, fused_body(): pl.pallas_call(apply, grid=(model // tile,), out_shape=own + [shape((mode...  12.1 us

profile of v3, /device:TPU:9, one launch (start us, length us, event | category | flops | bytes accessed | tf_op | source)
XLA Modules:
  0.0 129.7 jit_solution(12877227673334135607)
XLA Ops:
  0.6 117.0 %shard_map.195 = (f32[16,2048]{1,0:T(8,128)}, bf16[256,2048]{1,0:T(8,128)(2,1)}, bf16[2,2048,256]{2,1,0:T(8,128)(2,1)}, f32[2,8,128]{2,1,0:T(8,128)}, bf16[2048,...) custom-call(bf16[512,2048]{1,0:T(8,128)(2,1)} %input_hbm.1, bf16[512,1024]{1,0:T(8,128)(2,1)} %value_hbm.1, ...), custom_call_target="tpu_custom_call" | custom-call | tf_op jit(solution)/shard_map/pallas_call | solution.py:536
  117.7 12.1 %shard_map.196 = (f32[128,1024]{1,0:T(8,128)}, f32[1024,128]{1,0:T(8,128)}, f32[128,1024]{1,0:T(8,128)}, f32[1024,128]{1,0:T(8,128)}, f32[16,1024]{1,0:T(8,128)}...) custom-call(f32[16,2048]{1,0:T(8,128)} %get-tuple-element.16.low_ref, ...), custom_call_target="tpu_custom_call" | custom-call | tf_op jit(solution)/shard_map/pallas_call | solution.py:581
